TPU v7x, 32 devices: a whole 2x2x4 slice. The times are simulated.
32 devices in a mesh: grp: 2 (over y), fs: 4 (over z), tp: 4 (over x, core).
Axes of the slice: x: 2, y: 2, z: 4, core: 2. Of those that a mesh axis runs over, the one named last changes fastest.
Arguments:
- tokens: bfloat16 [8192, 2048], P(('grp', 'fs')), parts along dimension 0, may hold values from -6 to 6
- mixer_gain: float32 [2048], replicated, may hold values from 0.1 to 1.9
- outer_weight: float32 [2048, 2048], P('fs', 'tp'), may hold values from -0.125 to 0.125
- inner_weight: float32 [2048, 2048], P('fs', 'tp'), may hold values from -0.125 to 0.125
- value_weight: float32 [2048, 2048], P('fs', 'tp'), may hold values from -0.125 to 0.125
- filter_taps: float32 [3, 2048], P(None, 'tp'), may hold values from -3.5 to 3.5
- mixer_weight: float32 [2048, 2048], P('tp', 'fs'), may hold values from -0.125 to 0.125
- outer_scale: float32 [4, 512], P('tp', 'fs'), may hold values from 0.5 to 2
- inner_scale: float32 [4, 512], P('tp', 'fs'), may hold values from 0.5 to 2
- value_scale: float32 [4, 512], P('tp', 'fs'), may hold values from 0.5 to 2
- mixer_scale: float32 [1, 2048], P(None, 'fs'), may hold values from 0.5 to 2
Outputs:
- layer_out: bfloat16 [8192, 2048], P(('grp', 'fs', 'tp')), parts along dimension 0
There are 2 independent parts, one for each index of `grp`. A program takes and returns all parts, laid end to end along the dimension named above; an argument that names none is the same for every part. Nothing has to cross between parts.
All inputs are finite; a program needn't handle non-finite values.
Results may differ from a plain program's by a relative error of at most 0.014.
Values may be sent and summed in bfloat16 or wider, within the bound.
A program may use at most 64 MiB of HBM per device.

v0:
```python
import jax
import jax.numpy as jnp
from jax import lax
from jax.sharding import PartitionSpec as P

EPS = 1e-06


def normed(rows, gain):
    values = rows.astype(jnp.float32)
    inverse = lax.rsqrt(jnp.mean(values * values, axis=-1, keepdims=True) + EPS)
    return (values * inverse * gain).astype(jnp.bfloat16)


def rounded(values):
    return lax.optimization_barrier(values.astype(jnp.bfloat16)).astype(jnp.float32)


def add_rows(left, piece):
    return jnp.dot(left, piece, preferred_element_type=jnp.float32)


def per_device(
    tokens,
    mixer_gain,
    outer_weight,
    inner_weight,
    value_weight,
    filter_taps,
    mixer_weight,
    outer_scale,
    inner_scale,
    value_scale,
    mixer_scale,
):
    gathered = (
        lax.all_gather(outer_scale, "fs", axis=1, tiled=True),
        lax.all_gather(inner_scale, "fs", axis=1, tiled=True),
        lax.all_gather(value_scale, "fs", axis=1, tiled=True),
        lax.all_gather(mixer_scale, "fs", axis=1, tiled=True),
    )
    outer_col, inner_col, value_col, mixer_col = [piece.reshape(-1) for piece in gathered]
    seq_rows = tokens.shape[0]
    normal_rows = normed(tokens, mixer_gain)

    def fold_one(piece):
        return add_rows(normal_rows, piece)

    outer_sum = fold_one(
        lax.all_gather(outer_weight.astype(jnp.bfloat16), "fs", axis=0, tiled=True)
    )
    inner_sum = fold_one(
        lax.all_gather(inner_weight.astype(jnp.bfloat16), "fs", axis=0, tiled=True)
    )
    value_sum = fold_one(
        lax.all_gather(value_weight.astype(jnp.bfloat16), "fs", axis=0, tiled=True)
    )
    outer = rounded(outer_sum * outer_col)
    inner = rounded(inner_sum * inner_col)
    value = rounded(value_sum * value_col)
    padded = jnp.pad(inner * value, ((2, 0), (0, 0)))
    filtered = (
        filter_taps[0] * padded[0:seq_rows]
        + filter_taps[1] * padded[1 : seq_rows + 1]
        + filter_taps[2] * padded[2:]
    )
    gated = (outer * filtered).astype(jnp.bfloat16)
    mixer_full = lax.all_gather(mixer_weight.astype(jnp.bfloat16), "fs", axis=1, tiled=True)
    return lax.psum_scatter(
        (jnp.dot(gated, mixer_full, preferred_element_type=jnp.float32) * mixer_col).astype(
            jnp.bfloat16
        ),
        "tp",
        scatter_dimension=0,
        tiled=True,
    )


def solution(mesh):
    in_specs = (
        P(("grp", "fs"), None),
        P(),
        P("fs", "tp"),
        P("fs", "tp"),
        P("fs", "tp"),
        P(None, "tp"),
        P("tp", "fs"),
        P("tp", "fs"),
        P("tp", "fs"),
        P("tp", "fs"),
        P(None, "fs"),
    )
    out_specs = P(("grp", "fs", "tp"), None)
    return jax.shard_map(
        per_device, mesh=mesh, in_specs=in_specs, out_specs=out_specs, check_vma=False
    )
```

profile of v0, /device:TPU:0, one launch (start us, length us, event | category | flops | bytes accessed | tf_op | source)
XLA Modules:
  0.0 252.3 jit_solution(7031129598482165264)
XLA Ops:
  6.5 2.2 convert_element_type.46
  8.8 0.0 all-gather.5.cloned.1.call-update
  8.8 0.0 all-gather.7.cloned.1.call-start
  8.9 0.9 convert_element_type.49
  9.8 0.0 all-gather.9.cloned.1.call-start
  9.9 0.9 convert_element_type.52
  10.8 0.0 all-gather.11.cloned.1.call-start
  10.8 0.9 convert_element_type.56
  11.8 0.0 reduce-scatter.2.cloned.1.call-start
  11.8 12.7 %all_gather.25 = f32[1,512]{1,0:T(1,128)S(1)} all-gather(f32[1,128]{1,0:T(1,128)S(1)} %copy-done.5), channel_id=1, replica_groups=mesh['grp'=2,'fs'=4,'tp'=4] {'fs'}, dimensions={1}, use_global_device_ids=true | all-gather | bytes 2560 | tf_op jit(solution)/shard_map/all_gather | solution.py:37
  24.6 7.9 %all_gather.27 = f32[1,512]{1,0:T(1,128)S(1)} all-gather(f32[1,128]{1,0:T(1,128)S(1)} %copy-done.6), channel_id=1, replica_groups=mesh['grp'=2,'fs'=4,'tp'=4] {'fs'}, dimensions={1}, use_global_device_ids=true | all-gather | bytes 2560 | tf_op jit(solution)/shard_map/all_gather | solution.py:38
  32.5 11.0 %all_gather.29 = f32[1,512]{1,0:T(1,128)S(1)} all-gather(f32[1,128]{1,0:T(1,128)S(1)} %copy-done.7), channel_id=1, replica_groups=mesh['grp'=2,'fs'=4,'tp'=4] {'fs'}, dimensions={1}, use_global_device_ids=true | all-gather | bytes 2560 | tf_op jit(solution)/shard_map/all_gather | solution.py:39
  43.5 12.6 %all_gather.31 = f32[1,2048]{1,0:T(1,128)S(1)} all-gather(f32[1,512]{1,0:T(1,128)S(1)} %copy-done.4), channel_id=1, replica_groups=mesh['grp'=2,'fs'=4,'tp'=4] {'fs'}, dimensions={1}, use_global_device_ids=true | all-gather | bytes 10240 | tf_op jit(solution)/shard_map/all_gather | solution.py:40
  56.2 3.1 %fusion = f32[1024]{0:T(1024)S(1)} fusion(bf16[1024,2048]{1,0:T(8,128)(2,1)} %param.11), kind=kLoop, calls=%fused_computation.2 | loop fusion | flops 6290432 | bytes 4198400 | tf_op jit(solution)/shard_map/reduce_sum | solution.py:11
  59.3 0.0 all-gather.5.cloned.1.call-done
  59.4 6.2 %multiply_convert_fusion.4 = bf16[1024,512]{1,0:T(8,128)(2,1)} fusion(bf16[2048,512]{1,0:T(8,128)(2,1)} %all-gather.5.cloned.1.call-done, f32[512]{0:T(512)S(1)} %bitcast.14, bf16[1024,2048]{1,0:T(8,128)(2,1)} %param.11, f32[2048]{0:T(1024)S(1)} %copy-done.8, f32[1024]{0:T(1024)S(1)} %add_rsqrt_fusion), kind=kOutput, calls=%fused_computation.10 | convolution fusion | flops 2156920832 | bytes 7354368 | tf_op jit(solution)/shard_map/dot_general | solution.py:20
  65.6 38.0 %all-gather.7.cloned.1.call-done = bf16[2048,512]{1,0:T(8,128)(2,1)} async-done(((bf16[512,512]{1,0:T(8,128)(2,1)}), bf16[2048,512]{1,0:T(8,128)(2,1)}) %all-gather.7.cloned.1.call-update) | async-done | bytes 2097168 | tf_op jit(solution)/shard_map/all_gather | solution.py:53
  103.6 5.2 %multiply_convert_fusion.3 = bf16[1024,512]{1,0:T(8,128)(2,1)S(1)} fusion(bf16[2048,512]{1,0:T(8,128)(2,1)} %all-gather.7.cloned.1.call-done, f32[512]{0:T(512)S(1)} %bitcast.13, bf16[1024,2048]{1,0:T(8,128)(2,1)} %param.11, f32[2048]{0:T(1024)S(1)} %copy-done.8, f32[1024]{0:T(1024)S(1)} %add_rsqrt_fusion), kind=kOutput, calls=%fused_computation.9 | convolution fusion | flops 2156920832 | bytes 7354368 | tf_op jit(solution)/shard_map/dot_general | solution.py:20
  108.8 40.8 %all-gather.9.cloned.1.call-done = bf16[2048,512]{1,0:T(8,128)(2,1)} async-done(((bf16[512,512]{1,0:T(8,128)(2,1)}), bf16[2048,512]{1,0:T(8,128)(2,1)}) %all-gather.9.cloned.1.call-update) | async-done | bytes 2097168 | tf_op jit(solution)/shard_map/all_gather | solution.py:56
  149.7 5.2 %multiply_convert_fusion.2 = bf16[1024,512]{1,0:T(8,128)(2,1)S(1)} fusion(bf16[2048,512]{1,0:T(8,128)(2,1)} %all-gather.9.cloned.1.call-done, f32[512]{0:T(512)S(1)} %bitcast.12, bf16[1024,2048]{1,0:T(8,128)(2,1)} %param.11, f32[2048]{0:T(1024)S(1)} %copy-done.8, f32[1024]{0:T(1024)S(1)} %add_rsqrt_fusion), kind=kOutput, calls=%fused_computation.8 | convolution fusion | flops 2156920832 | bytes 7354368 | tf_op jit(solution)/shard_map/dot_general | solution.py:20
  154.9 0.3 convert_multiply_fusion.2
  155.2 40.4 %all-gather.11.cloned.1.call-done = bf16[512,2048]{1,0:T(8,128)(2,1)} async-done(((bf16[512,512]{1,0:T(8,128)(2,1)}), bf16[512,2048]{1,0:T(8,128)(2,1)}) %all-gather.11.cloned.1.call-update) | async-done | bytes 2097168 | tf_op jit(solution)/shard_map/all_gather | solution.py:68
  195.6 6.6 %multiply_convert_fusion = bf16[1024,2048]{1,0:T(8,128)(2,1)} fusion(bf16[512,2048]{1,0:T(8,128)(2,1)} %all-gather.11.cloned.1.call-done, f32[2048]{0:T(1024)S(1)} %bitcast.11, f32[1024,512]{1,0:T(8,128)S(1)} %convert_multiply_fusion.2, bf16[1024,512]{1,0:T(8,128)(2,1)} %multiply_convert_fusion.4, f32[512]{0:T(512)S(1)} %bitcast.16, f32[512]{0:T(512)S(1)} %bitcast.17, ...), kind=kOutput, calls=%fused_computation.5 | convolution fusion | flops 2155872256 | bytes 9451520 | tf_op jit(solution)/shard_map/dot_general | solution.py:70
  202.2 43.6 %reduce-scatter.2.cloned.1.call-done = bf16[256,2048]{1,0:T(8,128)(2,1)} async-done(((bf16[1024,2048]{1,0:T(8,128)(2,1)}), bf16[256,2048]{1,0:T(8,128)(2,1)}) %reduce-scatter.2.cloned.1.call-update) | async-done | bytes 1048592 | tf_op jit(solution)/shard_map/reduce_scatter | solution.py:69
  (25 shorter events, 0.1 us)
Async XLA Ops:
  6.5 2.3 copy-start
  6.5 3.3 %copy-start.1 = (f32[512,512]{1,0:T(8,128)S(1)}, f32[512,512]{1,0:T(8,128)}, u32[]{:S(2)}) copy-start(f32[512,512]{1,0:T(8,128)} %param.15) | copy-start | bytes 3145732
  6.5 52.8 %all-gather.5.cloned.1.call-start = ((), (), s32[]{:S(2)}) async-start(), calls=%async_computation.1 | async-start | bytes 2621440 | tf_op jit(solution)/shard_map/all_gather | solution.py:50
  8.8 2.0 copy-start.2
  8.8 94.8 %all-gather.7.cloned.1.call-start = ((), (), s32[]{:S(2)}) async-start(), calls=%async_computation.2 | async-start | bytes 2621440 | tf_op jit(solution)/shard_map/all_gather | solution.py:53
  9.8 2.1 copy-start.5
  9.8 14.8 %copy-start.6 = (f32[1,128]{1,0:T(1,128)S(1)}, f32[1,128]{1,0:T(1,128)}, u32[]{:S(2)}) copy-start(f32[1,128]{1,0:T(1,128)} %param.19) | copy-start | bytes 1540
  9.8 22.7 %copy-start.7 = (f32[1,128]{1,0:T(1,128)S(1)}, f32[1,128]{1,0:T(1,128)}, u32[]{:S(2)}) copy-start(f32[1,128]{1,0:T(1,128)} %param.20) | copy-start | bytes 1540
  9.8 33.7 %copy-start.4 = (f32[1,512]{1,0:T(1,128)S(1)}, f32[1,512]{1,0:T(1,128)}, u32[]{:S(2)}) copy-start(f32[1,512]{1,0:T(1,128)} %param.21) | copy-start | bytes 6148
  9.8 139.9 %all-gather.9.cloned.1.call-start = ((), (), s32[]{:S(2)}) async-start(), calls=%async_computation.3 | async-start | bytes 2621440 | tf_op jit(solution)/shard_map/all_gather | solution.py:56
  10.8 184.8 %all-gather.11.cloned.1.call-start = ((), (), s32[]{:S(2)}) async-start(), calls=%async_computation.4 | async-start | bytes 2621440 | tf_op jit(solution)/shard_map/all_gather | solution.py:68
  11.8 234.0 %reduce-scatter.2.cloned.1.call-start = ((), (), s32[]{:S(2)}) async-start(), calls=%async_computation.5 | async-start | bytes 5242880 | tf_op jit(solution)/shard_map/reduce_scatter | solution.py:69
  56.2 3.1 %copy-start.3 = (f32[3,512]{1,0:T(4,128)S(1)}, f32[3,512]{1,0:T(4,128)}, u32[]{:S(2)}) copy-start(f32[3,512]{1,0:T(4,128)} %param.16) | copy-start | bytes 18436
  56.2 3.2 %copy-start.8 = (f32[2048]{0:T(1024)S(1)}, f32[2048]{0:T(1024)}, u32[]{:S(2)}) copy-start(f32[2048]{0:T(1024)} %param.12) | copy-start | bytes 24580
Sparse Core Ops, SparseCore 0:
  8.9 48.5 all-gather.4
  59.1 44.4 all-gather.6
  105.2 44.4 all-gather.8
  151.1 44.4 all-gather.10
  202.3 43.3 reduce-scatter.1
where the time goes:
time: 252 us
  waiting for transfers between devices  163 us (65%)
  blocking collectives  44.3 us (18%)
  matrix products  23.3 us (9%)
  between operations  13.3 us (5%)
  other arithmetic  8.31 us (3%)
    reduce_scatter x1, waiting for transfers between devices, per_device(): lax.psum_scatter((jnp.dot(gated, mixer_full, preferred_element_type=jnp.f...  43.6 us
    all_gather x1, waiting for transfers between devices, per_device(): lax.all_gather(value_weight.astype(jnp.bfloat16), 'fs', axis=0, tiled=True)  40.8 us
    all_gather x1, waiting for transfers between devices, per_device(): lax.all_gather(mixer_weight.astype(jnp.bfloat16), 'fs', axis=1, tiled=True)  40.4 us
    all_gather x1, waiting for transfers between devices, per_device(): lax.all_gather(inner_weight.astype(jnp.bfloat16), 'fs', axis=0, tiled=True)  38 us
    dot_general x3, matrix products, add_rows(): return jnp.dot(left, piece, preferred_element_type=jnp.float32)  16.7 us
    all_gather x1, blocking collectives, per_device(): lax.all_gather(outer_scale, 'fs', axis=1, tiled=True)  12.7 us
    all_gather x1, blocking collectives, per_device(): lax.all_gather(mixer_scale, 'fs', axis=1, tiled=True)  12.6 us
    all_gather x1, blocking collectives, per_device(): lax.all_gather(value_scale, 'fs', axis=1, tiled=True)  11 us
  transfers between devices with their start and end apart: 5, of which 4 were waited for; matrix products, arithmetic and copies ran while one was open for 9% of the time, Pallas kernels for 0%

commit v1 on v0

--- a/solution.py
+++ b/solution.py
@@ -65,7 +65,7 @@
         + filter_taps[2] * padded[2:]
     )
     gated = (outer * filtered).astype(jnp.bfloat16)
-    mixer_full = lax.all_gather(mixer_weight.astype(jnp.bfloat16), "fs", axis=1, tiled=True)
+    mixer_full = jnp.concatenate(lax.all_gather(mixer_weight.astype(jnp.bfloat16), "fs"), axis=1)
     return lax.psum_scatter(
         (jnp.dot(gated, mixer_full, preferred_element_type=jnp.float32) * mixer_col).astype(
             jnp.bfloat16

time: 252 us -> 255 us (1.012)
  local copies, waits for them, and re-layouts: 0.05 us -> 2.84 us
    reshape x0 -> x1, local copies, waits for them, and re-layouts: none -> 2.79 us  [per_device(): jnp.concatenate(lax.all_gather(mixer_weight.astype(jnp.bfloat16), 'fs'),...]
where the time goes in v1:
time: 255 us
  waiting for transfers between devices  163 us (64%)
  blocking collectives  43.1 us (17%)
  matrix products  22.5 us (9%)
  between operations  13.3 us (5%)
  other arithmetic  9.65 us (4%)
  local copies, waits for them, and re-layouts  2.84 us (1%)
    reduce_scatter x1, waiting for transfers between devices, per_device(): lax.psum_scatter((jnp.dot(gated, mixer_full, preferred_element_type=jnp.f...  43.5 us
    all_gather x1, waiting for transfers between devices, per_device(): lax.all_gather(value_weight.astype(jnp.bfloat16), 'fs', axis=0, tiled=True)  40.8 us
    all_gather x1, waiting for transfers between devices, per_device(): lax.all_gather(mixer_weight.astype(jnp.bfloat16), 'fs')  39.7 us
    all_gather x1, waiting for transfers between devices, per_device(): lax.all_gather(inner_weight.astype(jnp.bfloat16), 'fs', axis=0, tiled=True)  39.2 us
    dot_general x3, matrix products, add_rows(): return jnp.dot(left, piece, preferred_element_type=jnp.float32)  17.8 us
    all_gather x1, blocking collectives, per_device(): lax.all_gather(outer_scale, 'fs', axis=1, tiled=True)  12.7 us
    all_gather x1, blocking collectives, per_device(): lax.all_gather(mixer_scale, 'fs', axis=1, tiled=True)  12.6 us
    all_gather x1, blocking collectives, per_device(): lax.all_gather(value_scale, 'fs', axis=1, tiled=True)  9.86 us
  transfers between devices with their start and end apart: 5, of which 4 were waited for; matrix products, arithmetic and copies ran while one was open for 9% of the time, Pallas kernels for 0%

profile of v1, /device:TPU:0, one launch (start us, length us, event | category | flops | bytes accessed | tf_op | source)
XLA Modules:
  0.0 254.8 jit_solution(9527864474918868912)
XLA Ops:
  6.5 2.3 convert_element_type.46
  8.9 0.0 all-gather.8.cloned.1.call-start
  8.9 0.9 convert_element_type.49
  9.9 0.0 all-gather.10.cloned.1.call-start
  10.0 0.9 convert_element_type.52
  10.8 0.0 all-gather.12.cloned.1.call-start
  10.9 0.9 convert_element_type.56
  11.8 0.0 reduce-scatter.2.cloned.1.call-start
  11.8 12.7 %all_gather.28 = f32[1,512]{1,0:T(1,128)S(1)} all-gather(f32[1,128]{1,0:T(1,128)S(1)} %copy-done.5), channel_id=1, replica_groups=mesh['grp'=2,'fs'=4,'tp'=4] {'fs'}, dimensions={1}, use_global_device_ids=true | all-gather | bytes 2560 | tf_op jit(solution)/shard_map/all_gather | solution.py:37
  24.6 7.9 %all_gather.30 = f32[1,512]{1,0:T(1,128)S(1)} all-gather(f32[1,128]{1,0:T(1,128)S(1)} %copy-done.6), channel_id=1, replica_groups=mesh['grp'=2,'fs'=4,'tp'=4] {'fs'}, dimensions={1}, use_global_device_ids=true | all-gather | bytes 2560 | tf_op jit(solution)/shard_map/all_gather | solution.py:38
  32.5 9.9 %all_gather.32 = f32[1,512]{1,0:T(1,128)S(1)} all-gather(f32[1,128]{1,0:T(1,128)S(1)} %copy-done.7), channel_id=1, replica_groups=mesh['grp'=2,'fs'=4,'tp'=4] {'fs'}, dimensions={1}, use_global_device_ids=true | all-gather | bytes 2560 | tf_op jit(solution)/shard_map/all_gather | solution.py:39
  42.4 12.6 %all_gather.35 = f32[1,2048]{1,0:T(1,128)S(1)} all-gather(f32[1,512]{1,0:T(1,128)S(1)} %copy-done.4), channel_id=1, replica_groups=mesh['grp'=2,'fs'=4,'tp'=4] {'fs'}, dimensions={1}, use_global_device_ids=true | all-gather | bytes 10240 | tf_op jit(solution)/shard_map/all_gather | solution.py:40
  55.0 3.1 %fusion = f32[1024]{0:T(1024)S(1)} fusion(bf16[1024,2048]{1,0:T(8,128)(2,1)} %param.11), kind=kLoop, calls=%fused_computation.2 | loop fusion | flops 6290432 | bytes 4198400 | tf_op jit(solution)/shard_map/reduce_sum | solution.py:11
  58.1 0.0 all-gather.6.cloned.1.call-done
  58.1 6.3 %multiply_convert_fusion.4 = bf16[1024,512]{1,0:T(8,128)(2,1)} fusion(bf16[2048,512]{1,0:T(8,128)(2,1)} %all-gather.6.cloned.1.call-done, f32[512]{0:T(512)S(1)} %bitcast.20, bf16[1024,2048]{1,0:T(8,128)(2,1)} %param.11, f32[2048]{0:T(1024)S(1)} %copy-done.8, f32[1024]{0:T(1024)S(1)} %add_rsqrt_fusion), kind=kOutput, calls=%fused_computation.10 | convolution fusion | flops 2156920832 | bytes 7354368 | tf_op jit(solution)/shard_map/dot_general | solution.py:20
  64.5 39.2 %all-gather.8.cloned.1.call-done = bf16[2048,512]{1,0:T(8,128)(2,1)} async-done(((bf16[512,512]{1,0:T(8,128)(2,1)}), bf16[2048,512]{1,0:T(8,128)(2,1)}) %all-gather.8.cloned.1.call-update) | async-done | bytes 2097168 | tf_op jit(solution)/shard_map/all_gather | solution.py:53
  103.7 5.3 %multiply_convert_fusion.3 = bf16[1024,512]{1,0:T(8,128)(2,1)S(1)} fusion(bf16[2048,512]{1,0:T(8,128)(2,1)} %all-gather.8.cloned.1.call-done, f32[512]{0:T(512)S(1)} %bitcast.19, bf16[1024,2048]{1,0:T(8,128)(2,1)} %param.11, f32[2048]{0:T(1024)S(1)} %copy-done.8, f32[1024]{0:T(1024)S(1)} %add_rsqrt_fusion), kind=kOutput, calls=%fused_computation.9 | convolution fusion | flops 2156920832 | bytes 7354368 | tf_op jit(solution)/shard_map/dot_general | solution.py:20
  108.9 40.8 %all-gather.10.cloned.1.call-done = bf16[2048,512]{1,0:T(8,128)(2,1)} async-done(((bf16[512,512]{1,0:T(8,128)(2,1)}), bf16[2048,512]{1,0:T(8,128)(2,1)}) %all-gather.10.cloned.1.call-update) | async-done | bytes 2097168 | tf_op jit(solution)/shard_map/all_gather | solution.py:56
  149.7 6.2 %multiply_convert_fusion.2 = bf16[1024,512]{1,0:T(8,128)(2,1)} fusion(bf16[2048,512]{1,0:T(8,128)(2,1)} %all-gather.10.cloned.1.call-done, f32[512]{0:T(512)S(1)} %bitcast.18, bf16[1024,2048]{1,0:T(8,128)(2,1)} %param.11, f32[2048]{0:T(1024)S(1)} %copy-done.8, f32[1024]{0:T(1024)S(1)} %add_rsqrt_fusion), kind=kOutput, calls=%fused_computation.8 | convolution fusion | flops 2156920832 | bytes 7354368 | tf_op jit(solution)/shard_map/dot_general | solution.py:20
  156.0 39.7 %all-gather.12.cloned.1.call-done = bf16[2048,512]{1,0:T(8,128)(2,1)} async-done(((bf16[512,512]{1,0:T(8,128)(2,1)}), bf16[2048,512]{1,0:T(8,128)(2,1)}) %all-gather.12.cloned.1.call-update) | async-done | bytes 2097168 | tf_op jit(solution)/shard_map/all_gather | solution.py:68
  195.7 2.8 %copy.12 = bf16[512,4,512]{0,2,1:T(8,128)(2,1)S(1)} copy(bf16[512,4,512]{2,0,1:T(8,128)(2,1)} %bitcast.15) | data formatting | bytes 4194304 | tf_op jit(solution)/shard_map/reshape | solution.py:68
  198.5 1.6 convert_multiply_fusion.2
  200.1 4.6 %multiply_convert_fusion = bf16[1024,2048]{1,0:T(8,128)(2,1)} fusion(bf16[512,2048]{0,1:T(8,128)(2,1)S(1)} %bitcast.16, f32[2048]{0:T(1024)S(1)} %bitcast.17, f32[1024,512]{1,0:T(8,128)S(1)} %convert_multiply_fusion.2, bf16[1024,512]{1,0:T(8,128)(2,1)S(1)} %copy-done.9, f32[512]{0:T(512)S(1)} %bitcast.22, f32[512]{0:T(512)S(1)} %bitcast.23, f32[512]{0:T(512)S(1)} %bitcast.21), kind=kOutput, calls=%fused_computation.5 | convolution fusion | flops 2155872256 | bytes 9451520 | tf_op jit(solution)/shard_map/dot_general | solution.py:70
  204.8 43.5 %reduce-scatter.2.cloned.1.call-done = bf16[256,2048]{1,0:T(8,128)(2,1)} async-done(((bf16[1024,2048]{1,0:T(8,128)(2,1)}), bf16[256,2048]{1,0:T(8,128)(2,1)}) %reduce-scatter.2.cloned.1.call-update) | async-done | bytes 1048592 | tf_op jit(solution)/shard_map/reduce_scatter | solution.py:69
  (28 shorter events, 0.1 us)
Async XLA Ops:
  6.5 2.4 copy-start
  6.5 3.4 %copy-start.1 = (f32[512,512]{1,0:T(8,128)S(1)}, f32[512,512]{1,0:T(8,128)}, u32[]{:S(2)}) copy-start(f32[512,512]{1,0:T(8,128)} %param.15) | copy-start | bytes 3145732
  6.5 51.6 %all-gather.6.cloned.1.call-start = ((), (), s32[]{:S(2)}) async-start(), calls=%async_computation.1 | async-start | bytes 2621440 | tf_op jit(solution)/shard_map/all_gather | solution.py:50
  8.9 2.0 copy-start.2
  8.9 94.8 %all-gather.8.cloned.1.call-start = ((), (), s32[]{:S(2)}) async-start(), calls=%async_computation.2 | async-start | bytes 2621440 | tf_op jit(solution)/shard_map/all_gather | solution.py:53
  9.8 2.0 copy-start.5
  9.9 14.7 %copy-start.6 = (f32[1,128]{1,0:T(1,128)S(1)}, f32[1,128]{1,0:T(1,128)}, u32[]{:S(2)}) copy-start(f32[1,128]{1,0:T(1,128)} %param.19) | copy-start | bytes 1540
  9.9 22.7 %copy-start.7 = (f32[1,128]{1,0:T(1,128)S(1)}, f32[1,128]{1,0:T(1,128)}, u32[]{:S(2)}) copy-start(f32[1,128]{1,0:T(1,128)} %param.20) | copy-start | bytes 1540
  9.9 32.5 %copy-start.4 = (f32[1,512]{1,0:T(1,128)S(1)}, f32[1,512]{1,0:T(1,128)}, u32[]{:S(2)}) copy-start(f32[1,512]{1,0:T(1,128)} %param.21) | copy-start | bytes 6148
  9.9 139.8 %all-gather.10.cloned.1.call-start = ((), (), s32[]{:S(2)}) async-start(), calls=%async_computation.3 | async-start | bytes 2621440 | tf_op jit(solution)/shard_map/all_gather | solution.py:56
  10.8 184.8 %all-gather.12.cloned.1.call-start = ((), (), s32[]{:S(2)}) async-start(), calls=%async_computation.5 | async-start | bytes 2621440 | tf_op jit(solution)/shard_map/all_gather | solution.py:68
  11.8 236.5 %reduce-scatter.2.cloned.1.call-start = ((), (), s32[]{:S(2)}) async-start(), calls=%async_computation.4 | async-start | bytes 5242880 | tf_op jit(solution)/shard_map/reduce_scatter | solution.py:69
  55.0 3.1 %copy-start.3 = (f32[3,512]{1,0:T(4,128)S(1)}, f32[3,512]{1,0:T(4,128)}, u32[]{:S(2)}) copy-start(f32[3,512]{1,0:T(4,128)} %param.16) | copy-start | bytes 18436
  55.0 3.2 %copy-start.8 = (f32[2048]{0:T(1024)S(1)}, f32[2048]{0:T(1024)}, u32[]{:S(2)}) copy-start(f32[2048]{0:T(1024)} %param.12) | copy-start | bytes 24580
  198.4 1.7 copy-start.9
Sparse Core Ops, SparseCore 0:
  9.0 48.5 all-gather.5
  59.2 44.4 all-gather.7
  105.2 44.4 all-gather.9
  151.2 44.4 all-gather.11
  204.9 43.3 reduce-scatter.1
